TPU v7x, 32 devices: a whole 2x2x4 slice. The times are simulated.
32 devices in a mesh: fs: 8 (over z, x), tp: 4 (over y, core).
Axes of the slice: x: 2, y: 2, z: 4, core: 2. Of those that a mesh axis runs over, the one named last changes fastest.
Arguments:
- tokens: bfloat16 [1024, 2048], P('fs'), may hold values from -6 to 6
- route_ids: int32 [1024, 2], P('fs'), may hold values from 0 to 15, as said below
- route_weights: float32 [1024, 2], P('fs'), may hold values from 0.05 to 0.6
- norm_gain: float32 [2048], P('fs'), may hold values from 0.1 to 1.9
- gate_weight: float32 [16, 2048, 1024], P(None, 'fs', 'tp'), may hold values from -6 to 6
- up_weight: float32 [16, 2048, 1024], P(None, 'fs', 'tp'), may hold values from -6 to 6
- down_weight: float32 [16, 2048, 1024], P(None, 'fs', 'tp'), may hold values from -6 to 6
Outputs:
- gate_served: bfloat16 [16, 2048, 1024], P('fs', None, 'tp')
- up_served: bfloat16 [16, 2048, 1024], P('fs', None, 'tp')
- down_served: bfloat16 [16, 2048, 1024], P('fs', None, 'tp')
- combined: bfloat16 [1024, 2048], P('fs', 'tp')
Inputs may be any that keep to these rules, and one draw needn't show every extreme that they name: `route_ids`: each row names 2 different experts of one group, numbers g * 4 to g * 4 + 3 for some g. In each aligned block of 128 rows (the rows of one index of fs) no expert is named by more than 32 rows, and some experts are named by exactly 32 rows in every block.
All inputs are finite; a program needn't handle non-finite values.
Results may differ from a plain program's by a relative error of at most 0.015.
Values may be sent and summed in bfloat16 or wider, within the bound.
A program may use at most 64 MiB of HBM per device.

v0:
```python
import jax
import jax.numpy as jnp
from jax import lax
from jax.sharding import PartitionSpec as P

GROUPS = 4
epsilon = 1e-06


def body(tokens, route_ids, route_weights, norm_gain, gate_weight, up_weight, down_weight):
    scaling = norm_gain[:, None]
    gate_folded = (scaling * gate_weight).astype(jnp.bfloat16)
    up_folded = (scaling * up_weight).astype(jnp.bfloat16)
    down_rounded = down_weight.astype(jnp.bfloat16)
    gate_served, up_served, down_served = (
        lax.all_to_all(gate_folded, "fs", split_axis=0, concat_axis=1, tiled=True),
        lax.all_to_all(up_folded, "fs", split_axis=0, concat_axis=1, tiled=True),
        lax.all_to_all(down_rounded, "fs", split_axis=0, concat_axis=1, tiled=True),
    )
    widened = tokens.astype(jnp.float32)
    normed = (
        widened * lax.rsqrt(jnp.mean(widened * widened, axis=1, keepdims=True) + epsilon)
    ).astype(jnp.bfloat16)
    tok_rows, d_model = tokens.shape
    routes = route_ids.shape[1]
    experts = gate_weight.shape[0]
    sources = lax.axis_size("fs")
    per_device = experts // sources
    capacity = tok_rows * GROUPS // experts
    flat_ids = route_ids.reshape(-1)
    onehot = (flat_ids[:, None] == jnp.arange(experts, dtype=jnp.int32)[None, :]).astype(jnp.int32)
    position = jnp.sum((jnp.cumsum(onehot, axis=0) - onehot) * onehot, axis=1)
    slot_index = (flat_ids * capacity + position).reshape(tok_rows, routes)
    token_of = jnp.repeat(jnp.arange(tok_rows, dtype=jnp.int32), routes)
    slot_token = (
        jnp.zeros((experts * capacity,), jnp.int32).at[slot_index.reshape(-1)].set(token_of)
    )
    hidden_local = gate_served.shape[2]
    col_width = d_model // lax.axis_size("tp")
    own_cols = lax.dynamic_slice_in_dim(normed, lax.axis_index("tp") * col_width, col_width, 1)
    arrived = lax.all_to_all(own_cols[slot_token], "fs", split_axis=0, concat_axis=0, tiled=True)
    arrived = arrived.reshape(sources, per_device, capacity, col_width)
    segment = lax.all_gather(arrived, "tp", axis=3, tiled=True)
    gate_more = jnp.einsum(
        "secd,edh->sech", segment, gate_served, preferred_element_type=jnp.float32
    )
    up_more = jnp.einsum("secd,edh->sech", segment, up_served, preferred_element_type=jnp.float32)
    input_scale = d_model ** (-0.5)
    hidden = (jax.nn.silu(gate_more * input_scale) * (up_more * input_scale)).astype(jnp.bfloat16)
    hidden_scale = (hidden_local * lax.axis_size("tp")) ** (-0.5)
    slots_here = sources * per_device * capacity
    partial_value = jnp.einsum(
        "edh,sech->dsec", down_served, hidden, preferred_element_type=jnp.float32
    )
    summed = lax.psum_scatter(
        (
            partial_value.reshape(
                lax.axis_size("tp") * (d_model // lax.axis_size("tp")), slots_here
            )
            * hidden_scale
        ).astype(jnp.bfloat16),
        "tp",
        scatter_dimension=0,
        tiled=True,
    )
    returned = lax.all_to_all(summed, "fs", split_axis=1, concat_axis=1, tiled=True)
    picked = jnp.take(returned, slot_index, axis=1).astype(jnp.float32)
    combined = jnp.einsum("dtk,tk->td", picked, route_weights, precision=lax.Precision.HIGHEST)
    return (gate_served, up_served, down_served, combined.astype(jnp.bfloat16))


def solution(mesh):
    placed = (
        P("fs", None),
        P("fs", None),
        P("fs", None),
        P("fs"),
        P(None, "fs", "tp"),
        P(None, "fs", "tp"),
        P(None, "fs", "tp"),
    )
    return jax.shard_map(
        body,
        mesh=mesh,
        in_specs=placed,
        out_specs=(P("fs", None, "tp"), P("fs", None, "tp"), P("fs", None, "tp"), P("fs", "tp")),
        check_vma=False,
    )
```

profile of v0, /device:TPU:0, one launch (start us, length us, event | category | flops | bytes accessed | tf_op | source)
XLA Modules:
  0.0 264.3 jit_solution(7585327871721887649)
XLA Ops:
  7.2 0.0 copy-start.2
  7.2 1.1 convert_element_type.43
  8.3 1.2 multiply_reduce_fusion
  9.6 0.0 copy-done.2
  9.6 0.1 copy.27
  9.7 0.1 eq.29
  9.8 0.1 eq.25
  10.0 0.6 reduce-window.6
  10.6 0.2 slice_reduce_fusion
  10.8 0.1 copy.32
  10.9 0.1 mul.85
  11.1 0.1 reshape.108
  11.2 0.1 fusion.19
  11.3 1.4 scatter_custom_fusion
  12.8 0.1 fusion.11
  12.8 0.0 copy-start.3
  12.9 2.6 gather_fusion
  15.5 7.3 %all-to-all-start.3 = ((bf16[8,64,512]{2,1,0:T(8,128)(2,1)}), bf16[8,64,512]{2,1,0:T(8,128)(2,1)S(1)}, u32[]{:S(2)}, u32[]{:S(2)}) async-start(bf16[8,64,512]{2,1,0:T(8,128)(2,1)} %bitcast.15), calls=%async_computation.3 | async-start | bytes 1048576 | tf_op jit(solution)/shard_map/all_to_all | solution.py:41
  22.8 0.0 copy-done.3
  22.8 5.8 %multiply_convert_fusion.1 = (bf16[16,256,256]{2,1,0:T(8,128)(2,1)}, bf16[16,256,256]{2,1,0:T(8,128)(2,1)S(1)}) fusion(f32[16,256,256]{2,1,0:T(8,128)} %param.12, f32[256]{0:T(256)S(1)} %copy-done.3, f32[16,256,256]{2,1,0:T(8,128)} %param.11), kind=kLoop, calls=%fused_computation.4 | loop fusion | flops 4194304 | bytes 12583936 | tf_op jit(solution)/shard_map/convert_element_type | solution.py:13
  28.6 8.7 %all-to-all-done.3 = bf16[8,64,512]{2,1,0:T(8,128)(2,1)S(1)} async-done(((bf16[8,64,512]{2,1,0:T(8,128)(2,1)}), bf16[8,64,512]{2,1,0:T(8,128)(2,1)S(1)}, u32[]{:S(2)}, u32[]{:S(2)}) %all-to-all-start.3) | async-done | bytes 524320 | tf_op jit(solution)/shard_map/all_to_all | solution.py:41
  37.3 51.9 %all_to_all.75 = bf16[16,256,256]{2,1,0:T(8,128)(2,1)} all-to-all(bf16[16,256,256]{2,1,0:T(8,128)(2,1)S(1)} %get-tuple-element.7), channel_id=1, replica_groups=mesh['fs'=8,'tp'=4] {'fs'}, dimensions={0} | all-to-all | bytes 4194304 | tf_op jit(solution)/shard_map/all_to_all | solution.py:16
  89.2 4.3 %all-to-all-start.1 = ((bf16[16,256,256]{2,1,0:T(8,128)(2,1)}), bf16[16,256,256]{2,1,0:T(8,128)(2,1)}, u32[]{:S(2)}, u32[]{:S(2)}) async-start(bf16[16,256,256]{2,1,0:T(8,128)(2,1)} %get-tuple-element.6), calls=%async_computation.1 | async-start | bytes 4194304 | tf_op jit(solution)/shard_map/all_to_all | solution.py:17
  93.5 3.8 %convert_element_type.40 = bf16[16,256,256]{2,1,0:T(8,128)(2,1)} convert(f32[16,256,256]{2,1,0:T(8,128)} %param.13) | non-fusion elementwise | flops 1048576 | bytes 6291456 | tf_op jit(solution)/shard_map/convert_element_type | solution.py:14
  97.3 0.0 copy-start
  97.3 43.5 %all-to-all-done.1 = bf16[16,256,256]{2,1,0:T(8,128)(2,1)} async-done(((bf16[16,256,256]{2,1,0:T(8,128)(2,1)}), bf16[16,256,256]{2,1,0:T(8,128)(2,1)}, u32[]{:S(2)}, u32[]{:S(2)}) %all-to-all-start.1) | async-done | bytes 2097184 | tf_op jit(solution)/shard_map/all_to_all | solution.py:17
  140.8 4.4 %all-to-all-start.2 = ((bf16[16,256,256]{2,1,0:T(8,128)(2,1)}), bf16[16,256,256]{2,1,0:T(8,128)(2,1)}, u32[]{:S(2)}, u32[]{:S(2)}) async-start(bf16[16,256,256]{2,1,0:T(8,128)(2,1)} %convert_element_type.40), calls=%async_computation.2 | async-start | bytes 4194304 | tf_op jit(solution)/shard_map/all_to_all | solution.py:18
  145.2 0.0 all-gather.2.cloned.1.call-start
  145.2 0.9 copy.33
  146.1 0.0 all-gather.2.cloned.1.call-update
  146.1 0.0 reduce-scatter.2.cloned.1.call-start
  146.2 0.0 copy-done
  146.2 1.5 copy.24
  147.6 3.1 %copy.25 = bf16[8,2,256,256]{3,2,0,1:T(8,128)(2,1)} copy(bf16[8,2,256,256]{3,2,1,0:T(8,128)(2,1)} %bitcast.3) | data formatting | bytes 4194304 | tf_op jit(solution)/shard_map/all_to_all | solution.py:17
  150.7 42.2 %all-to-all-done.2 = bf16[16,256,256]{2,1,0:T(8,128)(2,1)} async-done(((bf16[16,256,256]{2,1,0:T(8,128)(2,1)}), bf16[16,256,256]{2,1,0:T(8,128)(2,1)}, u32[]{:S(2)}, u32[]{:S(2)}) %all-to-all-start.2) | async-done | bytes 2097184 | tf_op jit(solution)/shard_map/all_to_all | solution.py:18
  193.0 0.0 copy-start.1
  193.0 3.2 %copy.26 = bf16[8,2,256,256]{3,2,0,1:T(8,128)(2,1)} copy(bf16[8,2,256,256]{3,2,1,0:T(8,128)(2,1)} %bitcast.6) | data formatting | bytes 4194304 | tf_op jit(solution)/shard_map/all_to_all | solution.py:18
  196.2 0.0 all-gather.2.cloned.1.call-done
  196.2 0.0 copy-done.1
  196.2 2.3 fusion.3
  198.5 4.2 %fusion = bf16[2048,8,2,32]{0,3,1,2:T(8,128)(2,1)S(1)} fusion(bf16[2,2048,256,1]{2,1,3,0:T(8,128)(2,1)} %bitcast.82, bf16[2,2048,256,1]{2,1,3,0:T(8,128)(2,1)} %bitcast.80, bf16[8,2,32,2048]{3,2,0,1:T(8,128)(2,1)} %all-gather.2.cloned.1.call-done, f32[8,2,32,256]{3,2,0,1:T(8,128)S(1)} %fusion.3), kind=kOutput, calls=%fused_computation.6 | convolution fusion | flops 1076756480 | bytes 8912896 | tf_op jit(solution)/shard_map/edh,sech->dsec/dot_general | solution.py:52
  202.8 1.5 copy.34
  204.2 0.0 copy-start.4
  204.2 0.0 reduce-scatter.2.cloned.1.call-update
  204.3 30.4 %reduce-scatter.2.cloned.1.call-done = bf16[512,512]{0,1:T(8,128)(2,1)} async-done(((bf16[2048,512]{0,1:T(8,128)(2,1)}), bf16[512,512]{0,1:T(8,128)(2,1)}) %reduce-scatter.2.cloned.1.call-update) | async-done | bytes 524304 | tf_op jit(solution)/shard_map/reduce_scatter | solution.py:55
  234.6 5.5 %all-to-all-start.4 = ((bf16[512,8,64]{0,2,1:T(8,128)(2,1)}), bf16[512,8,64]{0,2,1:T(8,128)(2,1)S(1)}, u32[]{:S(2)}, u32[]{:S(2)}) async-start(bf16[512,8,64]{0,2,1:T(8,128)(2,1)} %bitcast.85), calls=%async_computation.5 | async-start | bytes 1048576 | tf_op jit(solution)/shard_map/all_to_all | solution.py:66
  240.2 0.1 reduce_sum.23
  240.3 0.1 copy.30
  240.4 0.1 copy.35
  240.5 0.1 reshape.98
  240.6 0.1 copy.31
  240.8 0.0 copy-done.4
  240.8 0.1 copy.39
  240.9 13.6 %all-to-all-done.4 = bf16[512,8,64]{0,2,1:T(8,128)(2,1)S(1)} async-done(((bf16[512,8,64]{0,2,1:T(8,128)(2,1)}), bf16[512,8,64]{0,2,1:T(8,128)(2,1)S(1)}, u32[]{:S(2)}, u32[]{:S(2)}) %all-to-all-start.4) | async-done | bytes 524320 | tf_op jit(solution)/shard_map/all_to_all | solution.py:66
  254.5 1.2 gather_fusion.1
  255.6 0.1 reshape.101
  255.8 1.1 fusion.14
  256.8 0.7 copy.44
  (11 shorter events, 0.1 us)
Async XLA Ops:
  7.2 2.4 copy-start.2
  12.8 9.9 %copy-start.3 = (f32[256]{0:T(256)S(1)}, f32[256]{0:T(256)}, u32[]{:S(2)}) copy-start(f32[256]{0:T(256)} %param.10) | copy-start | bytes 3076
  15.5 21.8 %all-to-all-start.3 = ((bf16[8,64,512]{2,1,0:T(8,128)(2,1)}), bf16[8,64,512]{2,1,0:T(8,128)(2,1)S(1)}, u32[]{:S(2)}, u32[]{:S(2)}) async-start(bf16[8,64,512]{2,1,0:T(8,128)(2,1)} %bitcast.15), calls=%async_computation.3 | async-start | bytes 1048576 | tf_op jit(solution)/shard_map/all_to_all | solution.py:41
  89.2 51.6 %all-to-all-start.1 = ((bf16[16,256,256]{2,1,0:T(8,128)(2,1)}), bf16[16,256,256]{2,1,0:T(8,128)(2,1)}, u32[]{:S(2)}, u32[]{:S(2)}) async-start(bf16[16,256,256]{2,1,0:T(8,128)(2,1)} %get-tuple-element.6), calls=%async_computation.1 | async-start | bytes 4194304 | tf_op jit(solution)/shard_map/all_to_all | solution.py:17
  97.3 48.8 %copy-start = (bf16[16,256,256]{2,1,0:T(8,128)(2,1)S(1)}, bf16[16,256,256]{2,1,0:T(8,128)(2,1)}, u32[]{:S(2)}) copy-start(bf16[16,256,256]{2,1,0:T(8,128)(2,1)} %all_to_all.75) | copy-start | bytes 6291460
  140.8 52.2 %all-to-all-start.2 = ((bf16[16,256,256]{2,1,0:T(8,128)(2,1)}), bf16[16,256,256]{2,1,0:T(8,128)(2,1)}, u32[]{:S(2)}, u32[]{:S(2)}) async-start(bf16[16,256,256]{2,1,0:T(8,128)(2,1)} %convert_element_type.40), calls=%async_computation.2 | async-start | bytes 4194304 | tf_op jit(solution)/shard_map/all_to_all | solution.py:18
  145.2 51.0 %all-gather.2.cloned.1.call-start = ((), (), s32[]{:S(2)}) async-start(), calls=%async_computation.6 | async-start | bytes 2621440 | tf_op jit(solution)/shard_map/all_gather | solution.py:43
  146.1 88.5 %reduce-scatter.2.cloned.1.call-start = ((), (), s32[]{:S(2)}) async-start(), calls=%async_computation.7 | async-start | bytes 2621440 | tf_op jit(solution)/shard_map/reduce_scatter | solution.py:55
  193.0 3.3 %copy-start.1 = (bf16[8,2,256,256]{3,2,0,1:T(8,128)(2,1)S(1)}, bf16[8,2,256,256]{3,2,0,1:T(8,128)(2,1)}, u32[]{:S(2)}) copy-start(bf16[8,2,256,256]{3,2,0,1:T(8,128)(2,1)} %copy.24) | copy-start | bytes 6291460
  204.2 36.5 %copy-start.4 = (f32[128,2]{0,1:T(2,128)S(1)}, f32[128,2]{0,1:T(2,128)}, u32[]{:S(2)}) copy-start(f32[128,2]{0,1:T(2,128)} %param.9) | copy-start | bytes 3076
  234.6 19.8 %all-to-all-start.4 = ((bf16[512,8,64]{0,2,1:T(8,128)(2,1)}), bf16[512,8,64]{0,2,1:T(8,128)(2,1)S(1)}, u32[]{:S(2)}, u32[]{:S(2)}) async-start(bf16[512,8,64]{0,2,1:T(8,128)(2,1)} %bitcast.85), calls=%async_computation.5 | async-start | bytes 1048576 | tf_op jit(solution)/shard_map/all_to_all | solution.py:66
Sparse Core Ops, SparseCore 0:
  147.5 23.8 all-gather.1
  204.4 30.2 reduce-scatter.1
where the time goes:
time: 265 us; the launch traced here: 264 us
  waiting for transfers between devices  138 us (52%)
  blocking collectives  51.9 us (20%)
  starting transfers between devices  21.6 us (8%)
  local copies, waits for them, and re-layouts  17.8 us (7%)
  between operations  14.2 us (5%)
  other arithmetic  12.9 us (5%)
  matrix products  7.6 us (3%)
    all_to_all x1, blocking collectives, body(): lax.all_to_all(gate_folded, 'fs', split_axis=0, concat_axis=1, tiled=True)  51.9 us
    all_to_all x1, waiting for transfers between devices, body(): lax.all_to_all(up_folded, 'fs', split_axis=0, concat_axis=1, tiled=True)  43.5 us
    all_to_all x1, waiting for transfers between devices, body(): lax.all_to_all(down_rounded, 'fs', split_axis=0, concat_axis=1, tiled=True)  42.2 us
    reduce_scatter x1, waiting for transfers between devices, body(): lax.psum_scatter((partial_value.reshape(lax.axis_size('tp') * (d_model //...  30.4 us
    all_to_all x1, waiting for transfers between devices, body(): lax.all_to_all(summed, 'fs', split_axis=1, concat_axis=1, tiled=True)  13.6 us
    all_to_all x1, waiting for transfers between devices, body(): lax.all_to_all(own_cols[slot_token], 'fs', split_axis=0, concat_axis=0, t...  8.67 us
    all_to_all x1, starting transfers between devices, body(): lax.all_to_all(own_cols[slot_token], 'fs', split_axis=0, concat_axis=0, t...  7.28 us
    convert_element_type x1, other arithmetic, body(): up_folded = (scaling * up_weight).astype(jnp.bfloat16)  5.81 us
  transfers between devices with their start and end apart: 6, of which 5 were waited for; matrix products, arithmetic and copies ran while one was open for 7% of the time, Pallas kernels for 0%

commit v1 on v0

--- a/solution.py
+++ b/solution.py
@@ -5,6 +5,18 @@
 
 GROUPS = 4
 epsilon = 1e-06
+
+
+def split_up(x, dim, count):
+    dims = x.shape
+    blocks = x.reshape(*dims[:dim], count, dims[dim] // count, *dims[dim + 1 :])
+    return jnp.moveaxis(blocks, dim, 0)
+
+
+def in_order(blocks, dim):
+    shape = list(blocks.shape[1:])
+    shape[dim] *= blocks.shape[0]
+    return jnp.moveaxis(blocks, 0, dim).reshape(shape)
 
 
 def body(tokens, route_ids, route_weights, norm_gain, gate_weight, up_weight, down_weight):
@@ -38,7 +50,14 @@
     hidden_local = gate_served.shape[2]
     col_width = d_model // lax.axis_size("tp")
     own_cols = lax.dynamic_slice_in_dim(normed, lax.axis_index("tp") * col_width, col_width, 1)
-    arrived = lax.all_to_all(own_cols[slot_token], "fs", split_axis=0, concat_axis=0, tiled=True)
+    count, mine = (lax.axis_size("fs"), lax.axis_index("fs"))
+    blocks = split_up(own_cols[slot_token], 0, count)
+    outs = [blocks[mine]]
+    for turn in range(1, count):
+        sent = blocks[mine ^ turn]
+        outs.append(lax.ppermute(sent, "fs", [(i, i ^ turn) for i in range(count)]))
+    blocks = jnp.stack(outs)[mine ^ jnp.arange(count)]
+    arrived = in_order(blocks, 0)
     arrived = arrived.reshape(sources, per_device, capacity, col_width)
     segment = lax.all_gather(arrived, "tp", axis=3, tiled=True)
     gate_more = jnp.einsum(

time: 265 us -> 251 us (0.947)
  waiting for transfers between devices: 138 us -> 113 us
  starting transfers between devices: 21.6 us -> 30.1 us
  blocking collectives: 51.9 us -> 55.3 us
    all_to_all x1, waiting for transfers between devices: 43.5 us -> 0.01 us  [body(): lax.all_to_all(up_folded, 'fs', split_axis=0, concat_axis=1, tiled=True)]
    ppermute x0 -> x7, waiting for transfers between devices: none -> 29.2 us  [body(): outs.append(lax.ppermute(sent, 'fs', [(i, i ^ turn) for i in range(count)]))]
    ppermute x0 -> x7, starting transfers between devices: none -> 15.7 us  [body(): outs.append(lax.ppermute(sent, 'fs', [(i, i ^ turn) for i in range(count)]))]
    all_to_all x1 -> x0, waiting for transfers between devices: 8.67 us -> none  [body(): lax.all_to_all(own_cols[slot_token], 'fs', split_axis=0, concat_axis=0, t...]
    all_to_all x1 -> x0, starting transfers between devices: 7.28 us -> none  [body(): lax.all_to_all(own_cols[slot_token], 'fs', split_axis=0, concat_axis=0, t...]
    all_to_all x1, blocking collectives: 51.9 us -> 55.3 us  [body(): lax.all_to_all(gate_folded, 'fs', split_axis=0, concat_axis=1, tiled=True)]
  transfers between devices with their start and end apart: 6 -> 12, of which waited for: 5 -> 5; matrix products, arithmetic and copies ran while one was open for 7% -> 8% of each run, Pallas kernels for 0% -> 0%
where the time goes in v1:
time: 251 us
  waiting for transfers between devices  113 us (45%)
  blocking collectives  55.3 us (22%)
  starting transfers between devices  30.1 us (12%)
  local copies, waits for them, and re-layouts  17.8 us (7%)
  between operations  14.4 us (6%)
  other arithmetic  12.7 us (5%)
  matrix products  7.59 us (3%)
    all_to_all x1, blocking collectives, body(): lax.all_to_all(gate_folded, 'fs', split_axis=0, concat_axis=1, tiled=True)  55.3 us
    all_to_all x1, waiting for transfers between devices, body(): lax.all_to_all(down_rounded, 'fs', split_axis=0, concat_axis=1, tiled=True)  39.7 us
    reduce_scatter x1, waiting for transfers between devices, body(): lax.psum_scatter((partial_value.reshape(lax.axis_size('tp') * (d_model //...  30.2 us
    ppermute x7, waiting for transfers between devices, body(): outs.append(lax.ppermute(sent, 'fs', [(i, i ^ turn) for i in range(count)]))  29.2 us
    ppermute x7, starting transfers between devices, body(): outs.append(lax.ppermute(sent, 'fs', [(i, i ^ turn) for i in range(count)]))  15.7 us
    all_to_all x1, waiting for transfers between devices, body(): lax.all_to_all(summed, 'fs', split_axis=1, concat_axis=1, tiled=True)  13.6 us
    convert_element_type x1, other arithmetic, body(): up_folded = (scaling * up_weight).astype(jnp.bfloat16)  5.83 us
    all_to_all x1, starting transfers between devices, body(): lax.all_to_all(summed, 'fs', split_axis=1, concat_axis=1, tiled=True)  5.48 us
  transfers between devices with their start and end apart: 12, of which 5 were waited for; matrix products, arithmetic and copies ran while one was open for 8% of the time, Pallas kernels for 0%

profile of v1, /device:TPU:0, one launch (start us, length us, event | category | flops | bytes accessed | tf_op | source)
XLA Modules:
  0.0 250.6 jit_solution(5679863571891707232)
XLA Ops:
  7.2 5.8 %multiply_convert_fusion.1 = (bf16[16,256,256]{2,1,0:T(8,128)(2,1)}, bf16[16,256,256]{2,1,0:T(8,128)(2,1)S(1)}) fusion(f32[16,256,256]{2,1,0:T(8,128)} %param.12, f32[256]{0:T(256)} %param.10, f32[16,256,256]{2,1,0:T(8,128)} %param.11), kind=kLoop, calls=%fused_computation.5 | loop fusion | flops 4194304 | bytes 12583936 | tf_op jit(solution)/shard_map/convert_element_type | solution.py:25
  13.0 55.3 %all_to_all.66 = bf16[16,256,256]{2,1,0:T(8,128)(2,1)S(1)} all-to-all(bf16[16,256,256]{2,1,0:T(8,128)(2,1)S(1)} %get-tuple-element.15), channel_id=1, replica_groups=mesh['fs'=8,'tp'=4] {'fs'}, dimensions={0} | all-to-all | bytes 4194304 | tf_op jit(solution)/shard_map/all_to_all | solution.py:28
  68.3 4.5 %all-to-all-start.1 = ((bf16[16,256,256]{2,1,0:T(8,128)(2,1)}), bf16[16,256,256]{2,1,0:T(8,128)(2,1)}, u32[]{:S(2)}, u32[]{:S(2)}) async-start(bf16[16,256,256]{2,1,0:T(8,128)(2,1)} %get-tuple-element.14), calls=%async_computation.1 | async-start | bytes 4194304 | tf_op jit(solution)/shard_map/all_to_all | solution.py:29
  72.8 0.0 copy-done.2
  72.8 0.1 copy.27
  73.0 0.1 eq.29
  73.1 0.1 eq.25
  73.2 0.0 copy-done
  73.2 1.1 convert_element_type.43
  74.3 0.6 reduce-window.6
  74.9 0.2 slice_reduce_fusion
  75.1 0.1 copy.32
  75.2 0.1 mul.85
  75.4 0.1 reshape.129
  75.6 0.1 fusion.19
  75.7 1.4 scatter_custom_fusion
  77.1 0.2 multiply_reduce_fusion
  77.3 1.0 fusion.11
  78.4 2.0 gather_fusion
  80.3 0.1 dynamic-slice_bitcast_fusion
  80.4 1.9 collective-permute-start
  82.3 1.5 collective-permute-start.1
  83.8 0.2 collective-permute-start.2
  84.0 2.8 %collective-permute-start.3 = (bf16[64,512]{1,0:T(8,128)(2,1)S(1)}, bf16[64,512]{1,0:T(8,128)(2,1)S(1)}, u32[]{:S(2)}, u32[]{:S(2)}) collective-permute-start(bf16[64,512]{1,0:T(8,128)(2,1)S(1)} %get-tuple-element.9), channel_id=1, source_target_pairs={{0,16},{4,20},{8,24},{12,28},{16,0},{20,4},{24,8},{28,12},{1,17},{... | collective-permute-start | bytes 196616 | tf_op jit(solution)/shard_map/ppermute | solution.py:58
  86.7 1.4 collective-permute-start.4
  88.2 3.8 %convert_element_type.40 = bf16[16,256,256]{2,1,0:T(8,128)(2,1)} convert(f32[16,256,256]{2,1,0:T(8,128)} %param.13) | non-fusion elementwise | flops 1048576 | bytes 6291456 | tf_op jit(solution)/shard_map/convert_element_type | solution.py:26
  92.0 0.0 collective-permute-done
  92.0 3.4 %collective-permute-start.5 = (bf16[64,512]{1,0:T(8,128)(2,1)S(1)}, bf16[64,512]{1,0:T(8,128)(2,1)S(1)}, u32[]{:S(2)}, u32[]{:S(2)}) collective-permute-start(bf16[64,512]{1,0:T(8,128)(2,1)S(1)} %get-tuple-element.7), channel_id=1, source_target_pairs={{0,24},{4,28},{8,16},{12,20},{16,8},{20,12},{24,0},{28,4},{1,25},{... | collective-permute-start | bytes 196616 | tf_op jit(solution)/shard_map/ppermute | solution.py:58
  95.4 14.0 %collective-permute-done.1 = bf16[64,512]{1,0:T(8,128)(2,1)S(1)} collective-permute-done((bf16[64,512]{1,0:T(8,128)(2,1)S(1)}, bf16[64,512]{1,0:T(8,128)(2,1)S(1)}, u32[]{:S(2)}, u32[]{:S(2)}) %collective-permute-start.1) | collective-permute-done | bytes 65568 | tf_op jit(solution)/shard_map/ppermute | solution.py:58
  109.3 4.6 %collective-permute-start.6 = (bf16[64,512]{1,0:T(8,128)(2,1)S(1)}, bf16[64,512]{1,0:T(8,128)(2,1)S(1)}, u32[]{:S(2)}, u32[]{:S(2)}) collective-permute-start(bf16[64,512]{1,0:T(8,128)(2,1)S(1)} %get-tuple-element.6), channel_id=1, source_target_pairs={{0,28},{4,24},{8,20},{12,16},{16,12},{20,8},{24,4},{28,0},{1,29},{... | collective-permute-start | bytes 196616 | tf_op jit(solution)/shard_map/ppermute | solution.py:58
  113.9 0.0 collective-permute-done.2
  113.9 15.2 %collective-permute-done.3 = bf16[64,512]{1,0:T(8,128)(2,1)S(1)} collective-permute-done((bf16[64,512]{1,0:T(8,128)(2,1)S(1)}, bf16[64,512]{1,0:T(8,128)(2,1)S(1)}, u32[]{:S(2)}, u32[]{:S(2)}) %collective-permute-start.3) | collective-permute-done | bytes 65568 | tf_op jit(solution)/shard_map/ppermute | solution.py:58
  129.2 0.0 all-to-all-done.1
  129.2 4.4 %all-to-all-start.2 = ((bf16[16,256,256]{2,1,0:T(8,128)(2,1)}), bf16[16,256,256]{2,1,0:T(8,128)(2,1)}, u32[]{:S(2)}, u32[]{:S(2)}) async-start(bf16[16,256,256]{2,1,0:T(8,128)(2,1)} %convert_element_type.40), calls=%async_computation.2 | async-start | bytes 4194304 | tf_op jit(solution)/shard_map/all_to_all | solution.py:30
  133.5 0.0 all-gather.2.cloned.1.call-start
  133.6 0.0 collective-permute-done.4
  133.6 0.0 collective-permute-done.5
  133.6 0.0 collective-permute-done.6
  133.7 0.6 gather_fusion.1
  134.2 0.9 copy.33
  135.1 0.0 all-gather.2.cloned.1.call-update
  135.1 0.0 reduce-scatter.2.cloned.1.call-start
  135.2 1.5 copy.24
  136.7 3.1 %copy.25 = bf16[8,2,256,256]{3,2,0,1:T(8,128)(2,1)} copy(bf16[8,2,256,256]{3,2,1,0:T(8,128)(2,1)} %bitcast.3) | data formatting | bytes 4194304 | tf_op jit(solution)/shard_map/all_to_all | solution.py:29
  139.8 39.7 %all-to-all-done.2 = bf16[16,256,256]{2,1,0:T(8,128)(2,1)} async-done(((bf16[16,256,256]{2,1,0:T(8,128)(2,1)}), bf16[16,256,256]{2,1,0:T(8,128)(2,1)}, u32[]{:S(2)}, u32[]{:S(2)}) %all-to-all-start.2) | async-done | bytes 2097184 | tf_op jit(solution)/shard_map/all_to_all | solution.py:30
  179.4 3.2 %copy.26 = bf16[8,2,256,256]{3,2,0,1:T(8,128)(2,1)} copy(bf16[8,2,256,256]{3,2,1,0:T(8,128)(2,1)} %bitcast.6) | data formatting | bytes 4194304 | tf_op jit(solution)/shard_map/all_to_all | solution.py:30
  182.7 2.3 fusion.3
  185.0 4.2 %fusion = bf16[2048,8,2,32]{0,3,1,2:T(8,128)(2,1)S(1)} fusion(bf16[2,2048,256,1]{2,1,3,0:T(8,128)(2,1)} %bitcast.113, bf16[2,2048,256,1]{2,1,3,0:T(8,128)(2,1)} %bitcast.111, bf16[8,2,32,2048]{3,2,0,1:T(8,128)(2,1)} %all-gather.2.cloned.1.call-done, f32[8,2,32,256]{3,2,0,1:T(8,128)S(1)} %fusion.3), kind=kOutput, calls=%fused_computation.7 | convolution fusion | flops 1076756480 | bytes 8912896 | tf_op jit(solution)/shard_map/edh,sech->dsec/dot_general | solution.py:71
  189.2 1.5 copy.34
  190.7 0.0 reduce-scatter.2.cloned.1.call-update
  190.7 30.2 %reduce-scatter.2.cloned.1.call-done = bf16[512,512]{0,1:T(8,128)(2,1)} async-done(((bf16[2048,512]{0,1:T(8,128)(2,1)}), bf16[512,512]{0,1:T(8,128)(2,1)}) %reduce-scatter.2.cloned.1.call-update) | async-done | bytes 524304 | tf_op jit(solution)/shard_map/reduce_scatter | solution.py:74
  220.9 5.5 %all-to-all-start.3 = ((bf16[512,8,64]{0,2,1:T(8,128)(2,1)}), bf16[512,8,64]{0,2,1:T(8,128)(2,1)S(1)}, u32[]{:S(2)}, u32[]{:S(2)}) async-start(bf16[512,8,64]{0,2,1:T(8,128)(2,1)} %bitcast.116), calls=%async_computation.4 | async-start | bytes 1048576 | tf_op jit(solution)/shard_map/all_to_all | solution.py:85
  226.4 0.1 reduce_sum.23
  226.6 0.1 copy.30
  226.6 0.1 copy.35
  226.8 0.1 reshape.119
  226.9 0.1 copy.31
  227.0 0.0 copy-done.3
  227.1 0.1 copy.39
  227.2 13.6 %all-to-all-done.3 = bf16[512,8,64]{0,2,1:T(8,128)(2,1)S(1)} async-done(((bf16[512,8,64]{0,2,1:T(8,128)(2,1)}), bf16[512,8,64]{0,2,1:T(8,128)(2,1)S(1)}, u32[]{:S(2)}, u32[]{:S(2)}) %all-to-all-start.3) | async-done | bytes 524320 | tf_op jit(solution)/shard_map/all_to_all | solution.py:85
  240.8 1.2 gather_fusion.2
  241.9 0.1 reshape.122
  242.0 1.1 fusion.14
  243.1 0.7 copy.44
  (26 shorter events, 0.2 us)
Async XLA Ops:
  68.3 4.5 %copy-start.2 = (s32[128,2]{0,1:T(2,128)S(1)}, s32[128,2]{0,1:T(2,128)}, u32[]{:S(2)}) copy-start(s32[128,2]{0,1:T(2,128)} %param.8) | copy-start | bytes 3076
  68.3 4.9 %copy-start = (bf16[128,2048]{1,0:T(8,128)(2,1)S(1)}, bf16[128,2048]{1,0:T(8,128)(2,1)}, u32[]{:S(2)}) copy-start(bf16[128,2048]{1,0:T(8,128)(2,1)} %param.7) | copy-start | bytes 1572868
  68.3 60.9 %all-to-all-start.1 = ((bf16[16,256,256]{2,1,0:T(8,128)(2,1)}), bf16[16,256,256]{2,1,0:T(8,128)(2,1)}, u32[]{:S(2)}, u32[]{:S(2)}) async-start(bf16[16,256,256]{2,1,0:T(8,128)(2,1)} %get-tuple-element.14), calls=%async_computation.1 | async-start | bytes 4194304 | tf_op jit(solution)/shard_map/all_to_all | solution.py:29
  80.4 11.6 %collective-permute-start = (bf16[64,512]{1,0:T(8,128)(2,1)S(1)}, bf16[64,512]{1,0:T(8,128)(2,1)S(1)}, u32[]{:S(2)}, u32[]{:S(2)}) collective-permute-start(bf16[64,512]{1,0:T(8,128)(2,1)S(1)} %get-tuple-element.12), channel_id=1, source_target_pairs={{0,4},{4,0},{8,12},{12,8},{16,20},{20,16},{24,28},{28,24},{1,5},{5... | collective-permute-start | bytes 196616 | tf_op jit(solution)/shard_map/ppermute | solution.py:58
  82.3 27.0 %collective-permute-start.1 = (bf16[64,512]{1,0:T(8,128)(2,1)S(1)}, bf16[64,512]{1,0:T(8,128)(2,1)S(1)}, u32[]{:S(2)}, u32[]{:S(2)}) collective-permute-start(bf16[64,512]{1,0:T(8,128)(2,1)S(1)} %get-tuple-element.11), channel_id=1, source_target_pairs={{0,8},{4,12},{8,0},{12,4},{16,24},{20,28},{24,16},{28,20},{1,9},{5... | collective-permute-start | bytes 196616 | tf_op jit(solution)/shard_map/ppermute | solution.py:58
  83.8 30.1 %collective-permute-start.2 = (bf16[64,512]{1,0:T(8,128)(2,1)S(1)}, bf16[64,512]{1,0:T(8,128)(2,1)S(1)}, u32[]{:S(2)}, u32[]{:S(2)}) collective-permute-start(bf16[64,512]{1,0:T(8,128)(2,1)S(1)} %get-tuple-element.10), channel_id=1, source_target_pairs={{0,12},{4,8},{8,4},{12,0},{16,28},{20,24},{24,20},{28,16},{1,13},{... | collective-permute-start | bytes 196616 | tf_op jit(solution)/shard_map/ppermute | solution.py:58
  84.0 45.2 %collective-permute-start.3 = (bf16[64,512]{1,0:T(8,128)(2,1)S(1)}, bf16[64,512]{1,0:T(8,128)(2,1)S(1)}, u32[]{:S(2)}, u32[]{:S(2)}) collective-permute-start(bf16[64,512]{1,0:T(8,128)(2,1)S(1)} %get-tuple-element.9), channel_id=1, source_target_pairs={{0,16},{4,20},{8,24},{12,28},{16,0},{20,4},{24,8},{28,12},{1,17},{... | collective-permute-start | bytes 196616 | tf_op jit(solution)/shard_map/ppermute | solution.py:58
  86.7 46.9 %collective-permute-start.4 = (bf16[64,512]{1,0:T(8,128)(2,1)S(1)}, bf16[64,512]{1,0:T(8,128)(2,1)S(1)}, u32[]{:S(2)}, u32[]{:S(2)}) collective-permute-start(bf16[64,512]{1,0:T(8,128)(2,1)S(1)} %get-tuple-element.8), channel_id=1, source_target_pairs={{0,20},{4,16},{8,28},{12,24},{16,4},{20,0},{24,12},{28,8},{1,21},{... | collective-permute-start | bytes 196616 | tf_op jit(solution)/shard_map/ppermute | solution.py:58
  92.0 41.6 %collective-permute-start.5 = (bf16[64,512]{1,0:T(8,128)(2,1)S(1)}, bf16[64,512]{1,0:T(8,128)(2,1)S(1)}, u32[]{:S(2)}, u32[]{:S(2)}) collective-permute-start(bf16[64,512]{1,0:T(8,128)(2,1)S(1)} %get-tuple-element.7), channel_id=1, source_target_pairs={{0,24},{4,28},{8,16},{12,20},{16,8},{20,12},{24,0},{28,4},{1,25},{... | collective-permute-start | bytes 196616 | tf_op jit(solution)/shard_map/ppermute | solution.py:58
  109.3 24.3 %collective-permute-start.6 = (bf16[64,512]{1,0:T(8,128)(2,1)S(1)}, bf16[64,512]{1,0:T(8,128)(2,1)S(1)}, u32[]{:S(2)}, u32[]{:S(2)}) collective-permute-start(bf16[64,512]{1,0:T(8,128)(2,1)S(1)} %get-tuple-element.6), channel_id=1, source_target_pairs={{0,28},{4,24},{8,20},{12,16},{16,12},{20,8},{24,4},{28,0},{1,29},{... | collective-permute-start | bytes 196616 | tf_op jit(solution)/shard_map/ppermute | solution.py:58
  129.2 50.3 %all-to-all-start.2 = ((bf16[16,256,256]{2,1,0:T(8,128)(2,1)}), bf16[16,256,256]{2,1,0:T(8,128)(2,1)}, u32[]{:S(2)}, u32[]{:S(2)}) async-start(bf16[16,256,256]{2,1,0:T(8,128)(2,1)} %convert_element_type.40), calls=%async_computation.2 | async-start | bytes 4194304 | tf_op jit(solution)/shard_map/all_to_all | solution.py:30
  133.5 49.2 %all-gather.2.cloned.1.call-start = ((), (), s32[]{:S(2)}) async-start(), calls=%async_computation.5 | async-start | bytes 2621440 | tf_op jit(solution)/shard_map/all_gather | solution.py:62
  135.1 85.8 %reduce-scatter.2.cloned.1.call-start = ((), (), s32[]{:S(2)}) async-start(), calls=%async_computation.6 | async-start | bytes 2621440 | tf_op jit(solution)/shard_map/reduce_scatter | solution.py:74
  179.4 3.3 %copy-start.1 = (bf16[8,2,256,256]{3,2,0,1:T(8,128)(2,1)S(1)}, bf16[8,2,256,256]{3,2,0,1:T(8,128)(2,1)}, u32[]{:S(2)}) copy-start(bf16[8,2,256,256]{3,2,0,1:T(8,128)(2,1)} %copy.24) | copy-start | bytes 6291460
  190.7 36.3 %copy-start.3 = (f32[128,2]{0,1:T(2,128)S(1)}, f32[128,2]{0,1:T(2,128)}, u32[]{:S(2)}) copy-start(f32[128,2]{0,1:T(2,128)} %param.9) | copy-start | bytes 3076
  220.9 19.8 %all-to-all-start.3 = ((bf16[512,8,64]{0,2,1:T(8,128)(2,1)}), bf16[512,8,64]{0,2,1:T(8,128)(2,1)S(1)}, u32[]{:S(2)}, u32[]{:S(2)}) async-start(bf16[512,8,64]{0,2,1:T(8,128)(2,1)} %bitcast.116), calls=%async_computation.4 | async-start | bytes 1048576 | tf_op jit(solution)/shard_map/all_to_all | solution.py:85
Sparse Core Ops, SparseCore 0:
  135.9 23.8 all-gather.1
  190.9 30.0 reduce-scatter.1
